TPU v7x, 32 devices: a whole 2x2x4 slice. The times are simulated.
32 devices in a mesh: grp: 2 (over x), ep: 8 (over z, y), tp: 2 (over core).
Axes of the slice: x: 2, y: 2, z: 4, core: 2. Of those that a mesh axis runs over, the one named last changes fastest.
Arguments:
- tokens: bfloat16 [128, 1536], P(('grp', 'ep')), parts along dimension 0, may hold values from -6 to 6
- norm_gain: float32 [1536], replicated, may hold values from 0.1 to 1.9
- routes: int32 [128, 4], P(('grp', 'ep')), parts along dimension 0, may hold values from 0 to 7, all different within a row; in each aligned block of 8 rows (0 to 7, 8 to 15, ...) at most 8 rows name the same one
- route_weight: float32 [128, 4], P(('grp', 'ep')), parts along dimension 0, may hold values from 0.1 to 1
- expert_gate: bfloat16 [8, 1536, 1536], P('ep', None, 'tp'), may hold values from -2 to 2
- expert_up: bfloat16 [8, 1536, 1536], P('ep', None, 'tp'), may hold values from -2 to 2
- expert_down: bfloat16 [8, 1536, 1536], P('ep', 'tp'), may hold values from -0.0390625 to 0.0390625
- dense_gate: bfloat16 [1536, 4096], P(None, ('ep', 'tp')), may hold values from -2 to 2
- dense_up: bfloat16 [1536, 4096], P(None, ('ep', 'tp')), may hold values from -2 to 2
- dense_down: bfloat16 [4096, 1536], P(('ep', 'tp')), may hold values from -0.0234375 to 0.0234375
- gate_vector: bfloat16 [4096], P(('ep', 'tp')), may hold values from -0.0234375 to 0.0234375
Outputs:
- mixed: bfloat16 [128, 1536], P(('grp', 'ep'), 'tp'), parts along dimension 0
There are 2 independent parts, one for each index of `grp`. A program takes and returns all parts, laid end to end along the dimension named above; an argument that names none is the same for every part. Nothing has to cross between parts.
Inputs may be any that keep to these rules, and one draw needn't show every extreme that they name: `routes`: each token names 4 different experts. Within the rows of one index of ep (aligned blocks of 8 rows) no expert is named by more than 8 rows, a bound that some block reaches.
All inputs are finite; a program needn't handle non-finite values.
Results may differ from a plain program's by a relative error of at most 0.0077.
Values may be sent and summed in bfloat16 or wider, within the bound.
A program may use at most 64 MiB of HBM per device.

v0:
```python
import jax
import jax.numpy as jnp
from jax import lax
from jax.sharding import PartitionSpec as P

clamp_limit = 7.0
sigmoid_slope = 1.702
norm_eps = 1e-06


def clamped_unit(gate_pre, up_pre):
    gated = jnp.minimum(gate_pre, clamp_limit)
    linear = jnp.clip(up_pre, -clamp_limit, clamp_limit)
    return (gated * jax.nn.sigmoid(sigmoid_slope * gated) * (linear + 1.0)).astype(jnp.bfloat16)


def rms_normed(tokens, norm_gain):
    values = tokens.astype(jnp.float32)
    inverse = lax.rsqrt(jnp.mean(values * values, axis=-1, keepdims=True) + norm_eps)
    return (values * inverse * norm_gain).astype(jnp.bfloat16)


def per_device(
    tokens,
    norm_gain,
    routes,
    route_weight,
    expert_gate,
    expert_up,
    expert_down,
    dense_gate,
    dense_up,
    dense_down,
    gate_vector,
):
    tok_dev = tokens.shape[0]
    top_count = routes.shape[1]
    ep_count = lax.axis_size("ep")
    tp_count = lax.axis_size("tp")
    capacity = max(2, 2 * tok_dev * top_count // ep_count)
    slot_count = ep_count * capacity
    normed = rms_normed(tokens, norm_gain)
    flat_routes = routes.reshape(-1)
    member = (flat_routes[:, None] == jnp.arange(ep_count, dtype=jnp.int32)[None, :]).astype(
        jnp.int32
    )
    before = jnp.cumsum(member, axis=0) - member
    ranks_flat = jnp.sum(before * member, axis=1)
    slot_index = (flat_routes * capacity + ranks_flat).reshape(tok_dev, top_count)
    matched = slot_index[:, :, None] == jnp.arange(slot_count, dtype=jnp.int32)[None, None, :]
    dispatch = jnp.sum(matched.astype(jnp.float32), axis=1).astype(jnp.bfloat16)
    combine = jnp.sum(jnp.where(matched, route_weight[:, :, None], 0.0), axis=1)
    outgoing = jnp.einsum("ts,td->sd", dispatch, normed, preferred_element_type=jnp.float32).astype(
        jnp.bfloat16
    )
    arrived = lax.all_to_all(outgoing, "ep", split_axis=0, concat_axis=0, tiled=True)
    expert_act = clamped_unit(
        jnp.dot(arrived, expert_gate[0], preferred_element_type=jnp.float32),
        jnp.dot(arrived, expert_up[0], preferred_element_type=jnp.float32),
    )
    partial_value = jnp.dot(expert_act, expert_down[0], preferred_element_type=jnp.float32)
    summed = lax.psum_scatter(
        partial_value.astype(jnp.bfloat16), "tp", scatter_dimension=1, tiled=True
    )
    returned = lax.all_to_all(summed, "ep", split_axis=0, concat_axis=0, tiled=True)
    expert_mix = jnp.dot(combine, returned.astype(jnp.float32), precision=lax.Precision.HIGHEST)
    gate_cols, up_cols, vec_cols, down_rows = (dense_gate, dense_up, gate_vector, dense_down)
    block_rows = lax.all_gather(normed, "ep", axis=0, tiled=True)
    hidden = clamped_unit(
        jnp.dot(block_rows, gate_cols, preferred_element_type=jnp.float32),
        jnp.dot(block_rows, up_cols, preferred_element_type=jnp.float32),
    )
    logit_part = jnp.dot(hidden, vec_cols, preferred_element_type=jnp.float32)
    blocks = hidden.reshape(ep_count, tok_dev, hidden.shape[1])
    halves = down_rows.reshape(down_rows.shape[0], tp_count, down_rows.shape[1] // tp_count)
    term_rows = jnp.einsum("eth,hcd->ectd", blocks, halves, preferred_element_type=jnp.float32)
    logits = jnp.broadcast_to(
        logit_part.reshape(ep_count, 1, tok_dev), (ep_count, tp_count, tok_dev)
    )
    dense_out, gate_logit = (
        lax.psum_scatter(
            term_rows.reshape(-1, term_rows.shape[-1]),
            ("ep", "tp"),
            scatter_dimension=0,
            tiled=True,
        ),
        lax.psum_scatter(logits.reshape(-1), ("ep", "tp"), scatter_dimension=0, tiled=True),
    )
    mixed = jax.nn.sigmoid(gate_logit)[:, None] * dense_out + expert_mix
    return mixed.astype(jnp.bfloat16)


def solution(mesh):
    in_specs = (
        P(("grp", "ep"), None),
        P(),
        P(("grp", "ep"), None),
        P(("grp", "ep"), None),
        P("ep", None, "tp"),
        P("ep", None, "tp"),
        P("ep", "tp", None),
        P(None, ("ep", "tp")),
        P(None, ("ep", "tp")),
        P(("ep", "tp"), None),
        P(("ep", "tp")),
    )
    out_specs = P(("grp", "ep"), "tp")
    return jax.shard_map(
        per_device, mesh=mesh, in_specs=in_specs, out_specs=out_specs, check_vma=False
    )
```

profile of v0, /device:TPU:0, one launch (start us, length us, event | category | flops | bytes accessed | tf_op | source)
XLA Modules:
  0.0 136.1 jit_solution(17038698682080718248)
XLA Ops:
  6.5 0.0 copy-start
  6.5 0.9 copy.25
  7.4 0.1 eq.28
  7.5 0.1 fusion.51
  7.6 0.1 reduce_window_sum.11
  7.7 0.2 select_reduce_fusion.1
  7.8 0.1 reduce_sum.40
  7.9 0.1 copy.27
  8.0 0.9 fusion.47
  8.9 0.8 convert_reduce_fusion
  9.7 0.8 fusion.49
  10.5 0.9 fusion.9
  11.4 7.3 %all-to-all-start = ((bf16[8,8,1536]{2,1,0:T(8,128)(2,1)}), bf16[8,8,1536]{2,1,0:T(8,128)(2,1)S(1)}, u32[]{:S(2)}, u32[]{:S(2)}) async-start(bf16[8,8,1536]{2,1,0:T(8,128)(2,1)} %fusion.9), calls=%async_computation.1 | async-start | bytes 393216 | tf_op jit(solution)/shard_map/all_to_all | solution.py:56
  18.7 0.0 reduce-scatter.5.cloned.1.call-start
  18.8 32.1 %all_gather.3 = bf16[64,1536]{1,0:T(8,128)(2,1)S(1)} all-gather(bf16[8,1536]{1,0:T(8,128)(2,1)S(1)} %fusion.49), channel_id=1, replica_groups=mesh['grp'=2,'ep'=8,'tp'=2] {'ep'}, dimensions={0}, use_global_device_ids=true | all-gather | bytes 221184 | tf_op jit(solution)/shard_map/all_gather | solution.py:68
  50.8 2.0 %convolution_minimum_fusion = f32[64,256]{1,0:T(8,128)} fusion(bf16[64,1536]{1,0:T(8,128)(2,1)S(1)} %all_gather.3, bf16[1536,256]{1,0:T(8,128)(2,1)} %param.18), kind=kOutput, calls=%fused_computation.17 | convolution fusion | flops 50348032 | bytes 1048576 | tf_op jit(solution)/shard_map/dot_general | solution.py:70
  52.8 0.0 all-to-all-done
  52.8 2.9 %fusion.10 = f32[64,768]{1,0:T(8,128)} fusion(bf16[1,1536,768]{2,1,0:T(8,128)(2,1)} %param.15, bf16[8,8,1536]{2,1,0:T(8,128)(2,1)S(1)} %all-to-all-done), kind=kOutput, calls=%fused_computation.9 | convolution fusion | flops 151044096 | bytes 2752512 | tf_op jit(solution)/shard_map/dot_general | solution.py:58
  55.7 0.0 copy-done
  55.7 0.0 copy-start.1
  55.7 3.5 %fusion.6 = bf16[64,1536]{1,0:T(8,128)(2,1)} fusion(bf16[1,768,1536]{2,1,0:T(8,128)(2,1)S(1)} %copy-done, bf16[1,1536,768]{2,1,0:T(8,128)(2,1)} %param.16, bf16[8,8,1536]{2,1,0:T(8,128)(2,1)S(1)} %all-to-all-done, f32[64,768]{1,0:T(8,128)} %fusion.10), kind=kOutput, calls=%fused_computation.6 | convolution fusion | flops 302530560 | bytes 5308416 | tf_op jit(solution)/shard_map/dot_general | solution.py:61
  59.2 0.0 copy-start.2
  59.2 0.0 copy-start.3
  59.2 0.0 reduce-scatter.5.cloned.1.call-update
  59.3 0.0 reduce-scatter.3.cloned.1.call-start
  59.3 1.4 %fusion.27 = bf16[64,256]{1,0:T(8,128)(2,1)S(1)} fusion(bf16[64,1536]{1,0:T(8,128)(2,1)S(1)} %all_gather.3, bf16[1536,256]{1,0:T(8,128)(2,1)} %param.19, f32[64,256]{1,0:T(8,128)} %convolution_minimum_fusion), kind=kOutput, calls=%fused_computation.18 | convolution fusion | flops 50479104 | bytes 1081344 | tf_op jit(solution)/shard_map/dot_general | solution.py:71
  60.7 0.0 copy-done.1
  60.7 1.0 fusion.31
  61.7 0.0 reduce-scatter.3.cloned.1.call-update
  61.8 0.0 copy-done.2
  61.8 5.3 %reduce-scatter.5.cloned.1.call-done = bf16[64,768]{1,0:T(8,128)(2,1)} async-done(((bf16[64,1536]{1,0:T(8,128)(2,1)}), bf16[64,768]{1,0:T(8,128)(2,1)}) %reduce-scatter.5.cloned.1.call-update) | async-done | bytes 98320 | tf_op jit(solution)/shard_map/reduce_scatter | solution.py:62
  67.1 5.7 %all-to-all-start.1 = ((bf16[8,8,768]{2,1,0:T(8,128)(2,1)}), bf16[8,8,768]{2,1,0:T(8,128)(2,1)S(1)}, u32[]{:S(2)}, u32[]{:S(2)}) async-start(bf16[8,8,768]{2,1,0:T(8,128)(2,1)} %bitcast.66), calls=%async_computation.3 | async-start | bytes 196608 | tf_op jit(solution)/shard_map/all_to_all | solution.py:65
  72.8 0.1 convolution_bitcast_fusion
  72.9 0.1 broadcast_in_dim.16
  73.0 0.1 reshape.37
  73.1 0.0 copy-done.3
  73.2 0.6 dynamic-slice
  74.4 33.7 %all-reduce = f32[128]{0:T(128)S(1)} all-reduce(f32[128]{0:T(128)S(1)} %reshape.37), channel_id=2, replica_groups=mesh['grp'=2,'ep'=8,'tp'=2] {'ep','tp'}, use_global_device_ids=true, to_apply=%region_1.0.clone | all-reduce | flops 128 | bytes 1024
  108.1 0.1 add_divide_fusion
  108.2 19.6 %reduce-scatter.3.cloned.1.call-done = f32[8,768]{1,0:T(8,128)} async-done(((f32[128,768]{1,0:T(8,128)}), f32[8,768]{1,0:T(8,128)}) %reduce-scatter.3.cloned.1.call-update) | async-done | bytes 24592 | tf_op jit(solution)/shard_map/reduce_scatter | solution.py:81
  127.8 0.0 all-to-all-done.1
  127.8 1.5 %fusion.28 = bf16[8,768]{1,0:T(8,128)(2,1)} fusion(f32[8,64]{1,0:T(8,128)S(1)} %get-tuple-element.6, bf16[8,8,768]{2,1,0:T(8,128)(2,1)S(1)} %all-to-all-done.1, f32[8,768]{1,0:T(8,128)} %reduce-scatter.3.cloned.1.call-done, f32[8]{0:T(128)S(1)} %add_divide_fusion), kind=kOutput, calls=%fused_computation.20 | convolution fusion | flops 4737024 | bytes 137248 | tf_op jit(solution)/shard_map/dot_general | solution.py:66
  (4 shorter events, 0.0 us)
Async XLA Ops:
  6.5 49.2 %copy-start = (bf16[1,768,1536]{2,1,0:T(8,128)(2,1)S(1)}, bf16[1,768,1536]{2,1,0:T(8,128)(2,1)}, u32[]{:S(2)}) copy-start(bf16[1,768,1536]{2,1,0:T(8,128)(2,1)} %param.17) | copy-start | bytes 7077892
  11.4 41.4 %all-to-all-start = ((bf16[8,8,1536]{2,1,0:T(8,128)(2,1)}), bf16[8,8,1536]{2,1,0:T(8,128)(2,1)S(1)}, u32[]{:S(2)}, u32[]{:S(2)}) async-start(bf16[8,8,1536]{2,1,0:T(8,128)(2,1)} %fusion.9), calls=%async_computation.1 | async-start | bytes 393216 | tf_op jit(solution)/shard_map/all_to_all | solution.py:56
  18.7 48.4 %reduce-scatter.5.cloned.1.call-start = ((), (), s32[]{:S(2)}) async-start(), calls=%async_computation.5 | async-start | bytes 294912 | tf_op jit(solution)/shard_map/reduce_scatter | solution.py:62
  55.7 5.0 %copy-start.1 = (bf16[256,1536]{1,0:T(8,128)(2,1)S(1)}, bf16[256,1536]{1,0:T(8,128)(2,1)}, u32[]{:S(2)}) copy-start(bf16[256,1536]{1,0:T(8,128)(2,1)} %param.20) | copy-start | bytes 2359300
  59.2 2.5 %copy-start.2 = (bf16[256]{0:T(256)(128)(2,1)S(1)}, bf16[256]{0:T(256)(128)(2,1)}, u32[]{:S(2)}) copy-start(bf16[256]{0:T(256)(128)(2,1)} %param.21) | copy-start | bytes 1540
  59.2 13.9 %copy-start.3 = (u32[32]{0:T(128)S(1)}, u32[32]{0:T(128)}, u32[]{:S(2)}) copy-start(u32[32]{0:T(128)} %constant.36) | copy-start | bytes 388
  59.3 68.5 %reduce-scatter.3.cloned.1.call-start = ((), (), s32[]{:S(2)}) async-start(), calls=%async_computation.4 | async-start | bytes 417792 | tf_op jit(solution)/shard_map/reduce_scatter | solution.py:81
  67.1 60.7 %all-to-all-start.1 = ((bf16[8,8,768]{2,1,0:T(8,128)(2,1)}), bf16[8,8,768]{2,1,0:T(8,128)(2,1)S(1)}, u32[]{:S(2)}, u32[]{:S(2)}) async-start(bf16[8,8,768]{2,1,0:T(8,128)(2,1)} %bitcast.66), calls=%async_computation.3 | async-start | bytes 196608 | tf_op jit(solution)/shard_map/all_to_all | solution.py:65
Sparse Core Ops, SparseCore 0:
  59.4 7.6 reduce-scatter.4
  70.6 57.1 reduce-scatter.2
where the time goes:
time: 137 us; the launch traced here: 136 us
  blocking collectives  65.8 us (48%)
  waiting for transfers between devices  25 us (18%)
  between operations  14.1 us (10%)
  matrix products  13.3 us (10%)
  starting transfers between devices  13.1 us (10%)
  other arithmetic  2.87 us (2%)
  local copies, waits for them, and re-layouts  1.95 us (1%)
    unnamed x1, blocking collectives  33.7 us
    all_gather x1, blocking collectives, per_device(): block_rows = lax.all_gather(normed, 'ep', axis=0, tiled=True)  32.1 us
    reduce_scatter x1, waiting for transfers between devices, per_device(): lax.psum_scatter(term_rows.reshape(-1, term_rows.shape[-1]), ('ep', 'tp')...  19.6 us
    all_to_all x1, starting transfers between devices, per_device(): lax.all_to_all(outgoing, 'ep', split_axis=0, concat_axis=0, tiled=True)  7.31 us
    all_to_all x1, starting transfers between devices, per_device(): lax.all_to_all(summed, 'ep', split_axis=0, concat_axis=0, tiled=True)  5.71 us
    reduce_scatter x1, waiting for transfers between devices, per_device(): lax.psum_scatter(partial_value.astype(jnp.bfloat16), 'tp', scatter_dimens...  5.32 us
    dot_general x1, matrix products, per_device(): jnp.dot(expert_act, expert_down[0], preferred_element_type=jnp.float32)  3.52 us
    dot_general x1, matrix products, per_device(): jnp.dot(arrived, expert_gate[0], preferred_element_type=jnp.float32)  2.87 us
  transfers between devices with their start and end apart: 4, of which 2 were waited for; matrix products, arithmetic and copies ran while one was open for 4% of the time, Pallas kernels for 0%

commit v1 on v0

v1 whole, which is shorter than its diff:
```python
import functools

import jax
import jax.numpy as jnp
from jax import lax
from jax.experimental import pallas as pl
from jax.experimental.pallas import tpu as pltpu
from jax.sharding import PartitionSpec as P

MESH = pl.DeviceIdType.MESH
F32 = jnp.float32
BF16 = jnp.bfloat16
clamp_limit = 7.0
sigmoid_slope = 1.702
norm_eps = 1e-06
vmem_bytes = 67043328
extra = 128


def clamped_unit(gate_pre, up_pre):
    gated = jnp.minimum(gate_pre, clamp_limit)
    linear = jnp.clip(up_pre, -clamp_limit, clamp_limit)
    return (gated * jax.nn.sigmoid(sigmoid_slope * gated) * (linear + 1.0)).astype(BF16)


def split_lanes(value, shape):
    high = value.astype(BF16).astype(F32)
    middle = (value - high).astype(BF16).astype(F32)
    low = value - high - middle
    lane = lax.broadcasted_iota(jnp.int32, shape, len(shape) - 1)
    zero = jnp.zeros(shape, F32)
    out = jnp.where(lane == 0, high, jnp.where(lane == 1, middle, jnp.where(lane == 2, low, zero)))
    return out.astype(BF16)


def kernel(
    n, step,
    tok_hbm, gain_hbm, routes_hbm, weight_hbm, eg_hbm, eu_hbm, ed_hbm, dg_hbm, du_hbm, dd_hbm, gv_hbm,
    out_ref,
    tok, gain, routes, weight, gv, eg, eu, ed, dg, du, dd,
    x_mine, x_mate, acc_g, acc_u, acc_dg, acc_du, act, hidden, d_keep, e_keep, logit,
    d_give, d_take, d_out, d_in, e_give, e_take, e_out, e_in,
    small_sem, load_sem, x_send, x_recv, f_send, f_recv, d_send, d_recv, e_send, e_recv, p_send, p_recv,
):
    me, core = lax.axis_index("ep"), lax.axis_index("tp")
    mate = 1 - core
    rows, half = tok.shape[0], x_mine.shape[2]

    def peers(body):
        if n <= 16:
            order = sorted(range(1, n), key=lambda off: (abs(off - n + 2) % (n - 2), off))
            for off in order:
                body(lax.rem(me + off, n))
        else:
            def one(off, carry):
                body(lax.rem(me + off, n))
                return carry
            lax.fori_loop(1, n, one, 0)

    def chunks(body):
        if step == n:
            body(0)
        else:
            def one(index, carry):
                body(index * step)
                return carry
            lax.fori_loop(0, n // step, one, 0)

    def send(src, dst, ssem, rsem, device):
        return pltpu.make_async_remote_copy(
            src_ref=src, dst_ref=dst, send_sem=ssem, recv_sem=rsem,
            device_id=device, device_id_type=MESH,
        )

    barrier = pltpu.get_barrier_semaphore()
    peers(lambda p: pl.semaphore_signal(barrier, inc=1, device_id={"ep": p}, device_id_type=MESH))
    pl.semaphore_signal(barrier, inc=1, device_id={"tp": mate}, device_id_type=MESH)

    small = [
        pltpu.make_async_copy(src, dst, small_sem.at[i])
        for i, (src, dst) in enumerate(
            ((tok_hbm, tok), (gain_hbm, gain), (routes_hbm, routes), (weight_hbm, weight), (gv_hbm, gv))
        )
    ]
    for copy in small:
        copy.start()
    sides = (core, mate)
    loads = {}
    count = 0
    for name, src, dst, along in (
        ("dg", dg_hbm, dg, 0), ("du", du_hbm, du, 0), ("eg", eg_hbm.at[0], eg, 0),
        ("eu", eu_hbm.at[0], eu, 0), ("dd", dd_hbm, dd, 1), ("ed", ed_hbm.at[0], ed, 1),
    ):
        for k in range(2):
            cut = pl.ds(pl.multiple_of(sides[k] * half, 128), half)
            part = src.at[cut, :] if along == 0 else src.at[:, cut]
            loads[name, k] = pltpu.make_async_copy(part, dst.at[k], load_sem.at[count])
            count += 1
    for key in (("dg", 0), ("du", 0), ("eg", 0), ("eu", 0), ("dg", 1), ("du", 1), ("dd", 1), ("dd", 0),
                ("eg", 1), ("eu", 1), ("ed", 1), ("ed", 0)):
        loads[key].start()

    small[0].wait()
    small[1].wait()
    values = tok[...].astype(F32)
    inverse = lax.rsqrt(jnp.mean(values * values, axis=-1, keepdims=True) + norm_eps)
    normed = values * inverse * gain[...].reshape(1, 2 * half)
    left, right = normed[:, :half], normed[:, half:]
    first = core == 0
    x_mine[me] = jnp.where(first, left, right).astype(BF16)
    x_mate[me] = jnp.where(first, right, left).astype(BF16)

    pl.semaphore_wait(barrier, n)
    peers(lambda p: send(x_mine.at[me], x_mine.at[me], x_send.at[p], x_recv.at[me], {"ep": p}).start())

    def forward(p):
        send(x_mine.at[p], x_mine.at[p], x_send.at[p], x_recv.at[p], {"ep": p}).wait_recv()
        send(x_mine.at[p], x_mate.at[p], f_send.at[p], f_recv.at[p], {"tp": mate}).start()

    peers(forward)

    def at(ref, start):
        return pl.ds(start * rows, step * rows)

    def dot(a, b):
        return jnp.dot(a, b, preferred_element_type=F32)

    for key in (("dg", 0), ("du", 0), ("eg", 0), ("eu", 0)):
        loads[key].wait()

    def first_half(start):
        x = x_mine[pl.ds(start, step)].reshape(step * rows, half)
        cut = at(None, start)
        acc_dg[cut, :] = dot(x, dg[0])
        acc_du[cut, :] = dot(x, du[0])
        acc_g[cut, :] = dot(x, eg[0])
        acc_u[cut, :] = dot(x, eu[0])

    chunks(first_half)

    peers(lambda p: send(x_mine.at[p], x_mate.at[p], f_send.at[p], f_recv.at[p], {"tp": mate}).wait_recv())
    for key in (("dg", 1), ("du", 1), ("dd", 0), ("dd", 1)):
        loads[key].wait()
    small[4].wait()

    def dense(start):
        x = x_mate[pl.ds(start, step)].reshape(step * rows, half)
        cut = at(None, start)
        unit = clamped_unit(acc_dg[cut, :] + dot(x, dg[1]), acc_du[cut, :] + dot(x, du[1]))
        hidden[cut, :] = unit
        part = jnp.sum(unit.astype(F32) * gv[...].astype(F32).reshape(1, -1), axis=-1, keepdims=True)
        logit[cut, :] = jnp.broadcast_to(part, (step * rows, extra))
        away = dot(unit, dd[1]).astype(BF16)
        d_give[pl.ds(start, step), :, :half] = away.reshape(step, rows, half)
        lanes = split_lanes(part, (step * rows, extra))
        d_give[pl.ds(start, step), :, half:] = lanes.reshape(step, rows, extra)

    chunks(dense)
    d_pair = send(d_give, d_take, p_send.at[0], p_recv.at[0], {"tp": mate})
    d_pair.start()

    for key in (("eg", 1), ("eu", 1)):
        loads[key].wait()

    def expert(start):
        x = x_mate[pl.ds(start, step)].reshape(step * rows, half)
        cut = at(None, start)
        d_keep[cut, :] = dot(hidden[cut, :], dd[0])
        act[cut, :] = clamped_unit(acc_g[cut, :] + dot(x, eg[1]), acc_u[cut, :] + dot(x, eu[1]))

    chunks(expert)

    d_pair.wait_recv()

    def dense_sum(start):
        cut = at(None, start)
        took = d_take[pl.ds(start, step)].astype(F32).reshape(step * rows, half + extra)
        total = (d_keep[cut, :] + took[:, :half]).astype(BF16)
        d_out[pl.ds(start, step), :, :half] = total.reshape(step, rows, half)
        gate = logit[cut, :][:, :1] + jnp.sum(took[:, half:], axis=-1, keepdims=True)
        lanes = split_lanes(gate, (step * rows, extra))
        d_out[pl.ds(start, step), :, half:] = lanes.reshape(step, rows, extra)

    chunks(dense_sum)
    for key in (("ed", 1), ("ed", 0)):
        loads[key].wait()

    def give(start):
        away = dot(act[at(None, start), :], ed[1]).astype(BF16)
        e_give[pl.ds(start, step)] = away.reshape(step, rows, half)

    chunks(give)
    e_pair = send(e_give, e_take, p_send.at[1], p_recv.at[1], {"tp": mate})
    e_pair.start()
    peers(lambda p: send(d_out.at[p], d_in.at[me], d_send.at[p], d_recv.at[me], {"ep": p}).start())

    def keep(start):
        cut = at(None, start)
        e_keep[cut, :] = dot(act[cut, :], ed[0]).astype(BF16).astype(F32)

    chunks(keep)
    e_pair.wait_recv()

    def expert_sum(start):
        took = e_take[pl.ds(start, step)].astype(F32)
        own = e_keep[at(None, start), :].reshape(step, rows, half)
        e_out[pl.ds(start, step)] = (own + took).astype(BF16)

    chunks(expert_sum)
    peers(lambda p: send(e_out.at[p], e_in.at[me], e_send.at[p], e_recv.at[me], {"ep": p}).start())

    small[2].wait()
    small[3].wait()
    d_in[me] = d_out[me]
    e_in[me] = e_out[me]

    diagonal = lax.broadcasted_iota(jnp.int32, (rows, rows), 0) == lax.broadcasted_iota(
        jnp.int32, (rows, rows), 1
    )

    def column(row):
        return jnp.sum(jnp.where(diagonal, row, 0.0), axis=-1, keepdims=True)

    top = routes.shape[0]
    named = [column(routes[k : k + 1, :].astype(F32)) for k in range(top)]
    factor = [column(weight[k : k + 1, :]) for k in range(top)]

    def scaled(e):
        share = jnp.zeros((rows, 1), F32)
        for k in range(top):
            share = share + jnp.where(named[k] == jnp.asarray(e, F32), factor[k], 0.0)
        return share * e_in[e].astype(F32)

    peers(lambda p: send(d_out.at[p], d_in.at[p], d_send.at[p], d_recv.at[p], {"ep": p}).wait_recv())
    dense_all = jnp.sum(d_in[...].astype(F32), axis=0)
    gate_logit = jnp.sum(dense_all[:, half:], axis=-1, keepdims=True)
    base = jax.nn.sigmoid(gate_logit) * dense_all[:, :half]

    peers(lambda p: send(e_out.at[p], e_in.at[p], e_send.at[p], e_recv.at[p], {"ep": p}).wait_recv())
    if n <= 16:
        mix = scaled(0)
        for e in range(1, n):
            mix = mix + scaled(e)
    else:
        mix = lax.fori_loop(0, n, lambda e, total: total + scaled(e), jnp.zeros((rows, half), F32))
    out_ref[...] = (base + mix).astype(BF16)

    def sent(p):
        send(x_mine.at[me], x_mine.at[me], x_send.at[p], x_recv.at[me], {"ep": p}).wait_send()
        send(x_mine.at[p], x_mate.at[p], f_send.at[p], f_recv.at[p], {"tp": mate}).wait_send()
        send(d_out.at[p], d_in.at[me], d_send.at[p], d_recv.at[me], {"ep": p}).wait_send()
        send(e_out.at[p], e_in.at[me], e_send.at[p], e_recv.at[me], {"ep": p}).wait_send()

    peers(sent)
    d_pair.wait_send()
    e_pair.wait_send()


def solution(mesh):
    n, tp = mesh.shape["ep"], mesh.shape["tp"]
    assert tp == 2

    def per_device(
        tokens, norm_gain, routes, route_weight, expert_gate, expert_up, expert_down,
        dense_gate, dense_up, dense_down, gate_vector,
    ):
        rows, width = tokens.shape
        half = width // tp
        units, wide = expert_gate.shape[2], dense_gate.shape[1]
        step = min(n, 8)
        total = n * rows
        anywhere = pl.BlockSpec(memory_space=pltpu.HBM)
        vmem, dma = pltpu.VMEM, pltpu.SemaphoreType.DMA
        pieces = (n, rows, half)
        wider = (n, rows, half + extra)
        return pl.pallas_call(
            functools.partial(kernel, n, step),
            out_shape=jax.ShapeDtypeStruct((rows, half), BF16),
            in_specs=[anywhere] * 11,
            out_specs=pl.BlockSpec(memory_space=pltpu.VMEM),
            scratch_shapes=[
                vmem((rows, width), BF16), vmem((width,), F32),
                vmem(routes.shape[::-1], jnp.int32), vmem(route_weight.shape[::-1], F32), vmem((wide,), BF16),
                vmem((2, half, units), BF16), vmem((2, half, units), BF16), vmem((2, units, half), BF16),
                vmem((2, half, wide), BF16), vmem((2, half, wide), BF16), vmem((2, wide, half), BF16),
                vmem(pieces, BF16), vmem(pieces, BF16),
                vmem((total, units), F32), vmem((total, units), F32),
                vmem((total, wide), F32), vmem((total, wide), F32),
                vmem((total, units), BF16), vmem((total, wide), BF16),
                vmem((total, half), F32), vmem((total, half), F32), vmem((total, extra), F32),
                vmem(wider, BF16), vmem(wider, BF16), vmem(wider, BF16), vmem(wider, BF16),
                vmem(pieces, BF16), vmem(pieces, BF16), vmem(pieces, BF16), vmem(pieces, BF16),
                dma((5,)), dma((12,)),
                dma((n,)), dma((n,)), dma((n,)), dma((n,)), dma((n,)), dma((n,)), dma((n,)), dma((n,)),
                dma((2,)), dma((2,)),
            ],
            compiler_params=pltpu.CompilerParams(
                collective_id=0, has_side_effects=True, vmem_limit_bytes=vmem_bytes
            ),
        )(
            tokens, norm_gain, routes.T, route_weight.T, expert_gate, expert_up,
            expert_down, dense_gate, dense_up, dense_down, gate_vector,
        )

    in_specs = (
        P(("grp", "ep"), None), P(), P(("grp", "ep"), None), P(("grp", "ep"), None),
        P("ep", None, "tp"), P("ep", None, "tp"), P("ep", "tp", None),
        P(None, ("ep", "tp")), P(None, ("ep", "tp")), P(("ep", "tp"), None), P(("ep", "tp")),
    )
    return jax.shard_map(
        per_device, mesh=mesh, in_specs=in_specs, out_specs=P(("grp", "ep"), "tp"), check_vma=False
    )
```

time: 137 us -> 23.2 us (0.17)
  blocking collectives: 65.8 us -> 0 us
  waiting for transfers between devices: 25 us -> 0 us
  Pallas kernels: 0 us -> 21.7 us
  between operations: 14.1 us -> 0.01 us
  matrix products: 13.3 us -> 0 us
  starting transfers between devices: 13.1 us -> 0 us
  other arithmetic: 2.87 us -> 0 us
    unnamed x1 -> x0, blocking collectives: 33.7 us -> none
    all_gather x1 -> x0, blocking collectives: 32.1 us -> none  [per_device(): block_rows = lax.all_gather(normed, 'ep', axis=0, tiled=True)]
    reduce_scatter x2 -> x0, waiting for transfers between devices: 24.9 us -> none  [the longest x1 19.6 us: per_device(): lax.psum_scatter(term_rows.reshape(-1, term_rows.shape[-1]), ('ep', 'tp')...]
    pallas_call x0 -> x1, Pallas kernels: none -> 21.7 us  [per_device(): pl.pallas_call(functools.partial(kernel, n, step), out_shape=jax.ShapeDty...]
    dot_general x8 -> x0, matrix products: 13.3 us -> none  [the longest x1 3.52 us: per_device(): jnp.dot(expert_act, expert_down[0], preferred_element_type=jnp.float32)]
    all_to_all x2 -> x0, starting transfers between devices: 13 us -> none  [the longest x1 7.31 us: per_device(): lax.all_to_all(outgoing, 'ep', split_axis=0, concat_axis=0, tiled=True)]
    reduce_sum x3 -> x0, other arithmetic: 1.83 us -> none  [the longest x1 0.88 us: rms_normed(): jnp.mean(values * values, axis=-1, keepdims=True) + norm_eps]
  transfers between devices with their start and end apart: 4 -> 0, of which waited for: 2 -> 0; matrix products, arithmetic and copies ran while one was open for 4% -> 0% of each run, Pallas kernels for 0% -> 0%
where the time goes in v1:
time: 23.2 us; the launch traced here: 23 us
  Pallas kernels  21.7 us (94%)
  local copies, waits for them, and re-layouts  1.31 us (6%)
    pallas_call x1, Pallas kernels, per_device(): pl.pallas_call(functools.partial(kernel, n, step), out_shape=jax.ShapeDty...  21.7 us
    unnamed x1, local copies, waits for them, and re-layouts  1.31 us

profile of v1, /device:TPU:0, one launch (start us, length us, event | category | flops | bytes accessed | tf_op | source)
XLA Modules:
  0.0 23.0 jit_solution(7283567302913318464)
XLA Ops:
  0.0 21.7 %shard_map.109 = bf16[8,768]{1,0:T(8,128)(2,1)} custom-call(bf16[8,1536]{1,0:T(8,128)(2,1)} %tok_hbm.1, f32[1536]{0:T(1024)} %gain_hbm.1, s32[4,8]{1,0:T(4,128)} %bitcast.2, f32[4,8]{1,0:T(4,128)} %bitcast.3, bf16[1,1536,768]{2,1,0:T(8,128)(2,1)} %eg_hbm.1, bf16[1,1536,768]{2,1,0:T(8,128)(2,1)} %eu_hbm.1, bf16[1,768,1536]{2,1,0:T(8,128)(2,1)} %ed_hbm.1, ...), custom_call_target="tpu_custom_call" | custom-call | tf_op jit(solution)/shard_map/pallas_call | solution.py:276
  21.7 1.3 %copy.13 = bf16[8,768]{1,0:T(8,128)(2,1)} copy(bf16[8,768]{1,0:T(8,128)(2,1)} %shard_map.109) | data formatting | bytes 24576

commit v2 on v1

--- a/solution.py
+++ b/solution.py
@@ -13,7 +13,7 @@
 clamp_limit = 7.0
 sigmoid_slope = 1.702
 norm_eps = 1e-06
-vmem_bytes = 67043328
+vmem_bytes = 48 * 1024 * 1024
 extra = 128
 
 
@@ -46,10 +46,11 @@
     mate = 1 - core
     rows, half = tok.shape[0], x_mine.shape[2]
 
+    offsets = list(range(1, n))
+
     def peers(body):
         if n <= 16:
-            order = sorted(range(1, n), key=lambda off: (abs(off - n + 2) % (n - 2), off))
-            for off in order:
+            for off in offsets:
                 body(lax.rem(me + off, n))
         else:
             def one(off, carry):
@@ -182,6 +183,7 @@
         d_out[pl.ds(start, step), :, half:] = lanes.reshape(step, rows, extra)
 
     chunks(dense_sum)
+    peers(lambda p: send(d_out.at[p], d_in.at[me], d_send.at[p], d_recv.at[me], {"ep": p}).start())
     for key in (("ed", 1), ("ed", 0)):
         loads[key].wait()
 
@@ -192,7 +194,6 @@
     chunks(give)
     e_pair = send(e_give, e_take, p_send.at[1], p_recv.at[1], {"tp": mate})
     e_pair.start()
-    peers(lambda p: send(d_out.at[p], d_in.at[me], d_send.at[p], d_recv.at[me], {"ep": p}).start())
 
     def keep(start):
         cut = at(None, start)
@@ -236,24 +237,29 @@
     gate_logit = jnp.sum(dense_all[:, half:], axis=-1, keepdims=True)
     base = jax.nn.sigmoid(gate_logit) * dense_all[:, :half]
 
-    peers(lambda p: send(e_out.at[p], e_in.at[p], e_send.at[p], e_recv.at[p], {"ep": p}).wait_recv())
-    if n <= 16:
-        mix = scaled(0)
-        for e in range(1, n):
-            mix = mix + scaled(e)
-    else:
-        mix = lax.fori_loop(0, n, lambda e, total: total + scaled(e), jnp.zeros((rows, half), F32))
-    out_ref[...] = (base + mix).astype(BF16)
-
     def sent(p):
         send(x_mine.at[me], x_mine.at[me], x_send.at[p], x_recv.at[me], {"ep": p}).wait_send()
         send(x_mine.at[p], x_mate.at[p], f_send.at[p], f_recv.at[p], {"tp": mate}).wait_send()
         send(d_out.at[p], d_in.at[me], d_send.at[p], d_recv.at[me], {"ep": p}).wait_send()
-        send(e_out.at[p], e_in.at[me], e_send.at[p], e_recv.at[me], {"ep": p}).wait_send()
 
     peers(sent)
     d_pair.wait_send()
     e_pair.wait_send()
+
+    def arrived(p):
+        send(e_out.at[p], e_in.at[p], e_send.at[p], e_recv.at[p], {"ep": p}).wait_recv()
+
+    if n <= 16:
+        mix = base + scaled(me)
+        for off in offsets:
+            p = lax.rem(me + off, n)
+            arrived(p)
+            mix = mix + scaled(p)
+    else:
+        peers(arrived)
+        mix = lax.fori_loop(0, n, lambda e, total: total + scaled(e), base)
+    out_ref[...] = mix.astype(BF16)
+    peers(lambda p: send(e_out.at[p], e_in.at[me], e_send.at[p], e_recv.at[me], {"ep": p}).wait_send())
 
 
 def solution(mesh):
@@ -297,10 +303,10 @@
             compiler_params=pltpu.CompilerParams(
                 collective_id=0, has_side_effects=True, vmem_limit_bytes=vmem_bytes
             ),
-        )(
+        )(*[pltpu.with_memory_space_constraint(x, pltpu.HBM) for x in (
             tokens, norm_gain, routes.T, route_weight.T, expert_gate, expert_up,
             expert_down, dense_gate, dense_up, dense_down, gate_vector,
-        )
+        )])
 
     in_specs = (
         P(("grp", "ep"), None), P(), P(("grp", "ep"), None), P(("grp", "ep"), None),

time: 23.2 us -> 21.1 us (0.909)
  Pallas kernels: 21.7 us -> 20.3 us
  local copies, waits for them, and re-layouts: 1.31 us -> 0.6 us
    pallas_call x1, Pallas kernels: 21.7 us -> 20.3 us  [per_device(): pl.pallas_call(functools.partial(kernel, n, step), out_shape=jax.ShapeDty...]
    unnamed x1, local copies, waits for them, and re-layouts: 1.31 us -> 0.6 us
where the time goes in v2:
time: 21.1 us; the launch traced here: 20.9 us
  Pallas kernels  20.3 us (96%)
  local copies, waits for them, and re-layouts  0.6 us (3%)
    pallas_call x1, Pallas kernels, per_device(): pl.pallas_call(functools.partial(kernel, n, step), out_shape=jax.ShapeDty...  20.3 us
    unnamed x1, local copies, waits for them, and re-layouts  0.6 us

profile of v2, /device:TPU:0, one launch (start us, length us, event | category | flops | bytes accessed | tf_op | source)
XLA Modules:
  0.0 20.9 jit_solution(4508184847461092353)
XLA Ops:
  0.0 20.3 %shard_map.109 = bf16[8,768]{1,0:T(8,128)(2,1)S(1)} custom-call(bf16[8,1536]{1,0:T(8,128)(2,1)} %tok_hbm.1, f32[1536]{0:T(1024)} %gain_hbm.1, s32[4,8]{1,0:T(4,128)} %bitcast.2, f32[4,8]{1,0:T(4,128)} %bitcast.3, bf16[1,1536,768]{2,1,0:T(8,128)(2,1)} %eg_hbm.1, bf16[1,1536,768]{2,1,0:T(8,128)(2,1)} %eu_hbm.1, bf16[1,768,1536]{2,1,0:T(8,128)(2,1)} %ed_hbm.1, ...), custom_call_target="tpu_custom_call" | custom-call | tf_op jit(solution)/shard_map/pallas_call | solution.py:282
  20.3 0.6 %copy.13 = bf16[8,768]{1,0:T(8,128)(2,1)} copy(bf16[8,768]{1,0:T(8,128)(2,1)S(1)} %shard_map.109) | data formatting | bytes 24576

commit v3 on v2

--- a/solution.py
+++ b/solution.py
@@ -14,23 +14,12 @@
 sigmoid_slope = 1.702
 norm_eps = 1e-06
 vmem_bytes = 48 * 1024 * 1024
-extra = 128
 
 
 def clamped_unit(gate_pre, up_pre):
     gated = jnp.minimum(gate_pre, clamp_limit)
     linear = jnp.clip(up_pre, -clamp_limit, clamp_limit)
     return (gated * jax.nn.sigmoid(sigmoid_slope * gated) * (linear + 1.0)).astype(BF16)
-
-
-def split_lanes(value, shape):
-    high = value.astype(BF16).astype(F32)
-    middle = (value - high).astype(BF16).astype(F32)
-    low = value - high - middle
-    lane = lax.broadcasted_iota(jnp.int32, shape, len(shape) - 1)
-    zero = jnp.zeros(shape, F32)
-    out = jnp.where(lane == 0, high, jnp.where(lane == 1, middle, jnp.where(lane == 2, low, zero)))
-    return out.astype(BF16)
 
 
 def kernel(
@@ -38,20 +27,34 @@
     tok_hbm, gain_hbm, routes_hbm, weight_hbm, eg_hbm, eu_hbm, ed_hbm, dg_hbm, du_hbm, dd_hbm, gv_hbm,
     out_ref,
     tok, gain, routes, weight, gv, eg, eu, ed, dg, du, dd,
-    x_mine, x_mate, acc_g, acc_u, acc_dg, acc_du, act, hidden, d_keep, e_keep, logit,
+    x_mine, x_mate, acc_g, acc_u, acc_dg, acc_du, act, hidden, d_keep, e_keep, l_give, l_take, l_out, l_in,
     d_give, d_take, d_out, d_in, e_give, e_take, e_out, e_in,
     small_sem, load_sem, x_send, x_recv, f_send, f_recv, d_send, d_recv, e_send, e_recv, p_send, p_recv,
+    l_send, l_recv,
 ):
     me, core = lax.axis_index("ep"), lax.axis_index("tp")
     mate = 1 - core
     rows, half = tok.shape[0], x_mine.shape[2]
 
-    offsets = list(range(1, n))
-
-    def peers(body):
-        if n <= 16:
-            for off in offsets:
-                body(lax.rem(me + off, n))
+    paired = n % 2 == 0 and n <= 8
+    line = n // 2
+    place, side = me // 2, lax.rem(me, 2)
+    buddy = me + 1 - 2 * side
+
+    def nearby(k):
+        low = k + jnp.where(k >= place, 1, 0)
+        top = line - 1 - k
+        high = top - jnp.where(top <= place, 1, 0)
+        return jnp.where(2 * place < line, low, high)
+
+    def peers(body, far_first=False):
+        if paired:
+            order = [buddy]
+            for k in range(line - 1):
+                other = nearby(k)
+                order += [2 * other + side, 2 * other + 1 - side]
+            for p in order[::-1] if far_first else order:
+                body(p)
         else:
             def one(off, carry):
                 body(lax.rem(me + off, n))
@@ -74,8 +77,11 @@
         )
 
     barrier = pltpu.get_barrier_semaphore()
-    peers(lambda p: pl.semaphore_signal(barrier, inc=1, device_id={"ep": p}, device_id_type=MESH))
+    def tell(sem, p):
+        pl.semaphore_signal(sem, inc=1, device_id={"ep": p}, device_id_type=MESH)
+
     pl.semaphore_signal(barrier, inc=1, device_id={"tp": mate}, device_id_type=MESH)
+    peers(lambda p: tell(barrier, p))
 
     small = [
         pltpu.make_async_copy(src, dst, small_sem.at[i])
@@ -97,8 +103,7 @@
             part = src.at[cut, :] if along == 0 else src.at[:, cut]
             loads[name, k] = pltpu.make_async_copy(part, dst.at[k], load_sem.at[count])
             count += 1
-    for key in (("dg", 0), ("du", 0), ("eg", 0), ("eu", 0), ("dg", 1), ("du", 1), ("dd", 1), ("dd", 0),
-                ("eg", 1), ("eu", 1), ("ed", 1), ("ed", 0)):
+    for key in (("dg", 0), ("du", 0), ("eg", 0), ("eu", 0)):
         loads[key].start()
 
     small[0].wait()
@@ -111,12 +116,20 @@
     x_mine[me] = jnp.where(first, left, right).astype(BF16)
     x_mate[me] = jnp.where(first, right, left).astype(BF16)
 
+    def to_peer(p, source):
+        return send(x_mine.at[source], x_mine.at[source], x_send.at[p], x_recv.at[source], {"ep": p})
+
+    def peer_on(p):
+        return send(x_mine.at[p], x_mate.at[p], f_send.at[p], f_recv.at[p], {"tp": mate})
+
     pl.semaphore_wait(barrier, n)
-    peers(lambda p: send(x_mine.at[me], x_mine.at[me], x_send.at[p], x_recv.at[me], {"ep": p}).start())
+    peers(lambda p: to_peer(p, me).start(), True)
+    for key in (("dg", 1), ("du", 1), ("dd", 1), ("dd", 0), ("eg", 1), ("eu", 1), ("ed", 1), ("ed", 0)):
+        loads[key].start()
 
     def forward(p):
-        send(x_mine.at[p], x_mine.at[p], x_send.at[p], x_recv.at[p], {"ep": p}).wait_recv()
-        send(x_mine.at[p], x_mate.at[p], f_send.at[p], f_recv.at[p], {"tp": mate}).start()
+        to_peer(p, p).wait_recv()
+        peer_on(p).start()
 
     peers(forward)
 
@@ -139,7 +152,7 @@
 
     chunks(first_half)
 
-    peers(lambda p: send(x_mine.at[p], x_mate.at[p], f_send.at[p], f_recv.at[p], {"tp": mate}).wait_recv())
+    peers(lambda p: peer_on(p).wait_recv())
     for key in (("dg", 1), ("du", 1), ("dd", 0), ("dd", 1)):
         loads[key].wait()
     small[4].wait()
@@ -149,16 +162,17 @@
         cut = at(None, start)
         unit = clamped_unit(acc_dg[cut, :] + dot(x, dg[1]), acc_du[cut, :] + dot(x, du[1]))
         hidden[cut, :] = unit
-        part = jnp.sum(unit.astype(F32) * gv[...].astype(F32).reshape(1, -1), axis=-1, keepdims=True)
-        logit[cut, :] = jnp.broadcast_to(part, (step * rows, extra))
+        vector = jnp.broadcast_to(gv[...].astype(F32).reshape(1, -1), (8, unit.shape[1])).astype(BF16)
+        logits = lax.dot_general(vector, unit, (((1,), (1,)), ((), ())), preferred_element_type=F32)
+        l_give[:, pl.ds(pl.multiple_of(start * rows, step * rows), step * rows)] = logits[:1]
         away = dot(unit, dd[1]).astype(BF16)
-        d_give[pl.ds(start, step), :, :half] = away.reshape(step, rows, half)
-        lanes = split_lanes(part, (step * rows, extra))
-        d_give[pl.ds(start, step), :, half:] = lanes.reshape(step, rows, extra)
+        d_give[pl.ds(start, step)] = away.reshape(step, rows, half)
 
     chunks(dense)
     d_pair = send(d_give, d_take, p_send.at[0], p_recv.at[0], {"tp": mate})
     d_pair.start()
+    l_pair = send(l_give, l_take, p_send.at[2], p_recv.at[2], {"tp": mate})
+    l_pair.start()
 
     for key in (("eg", 1), ("eu", 1)):
         loads[key].wait()
@@ -172,18 +186,18 @@
     chunks(expert)
 
     d_pair.wait_recv()
+    l_pair.wait_recv()
+    l_out[...] = l_give[...] + l_take[...]
 
     def dense_sum(start):
         cut = at(None, start)
-        took = d_take[pl.ds(start, step)].astype(F32).reshape(step * rows, half + extra)
-        total = (d_keep[cut, :] + took[:, :half]).astype(BF16)
-        d_out[pl.ds(start, step), :, :half] = total.reshape(step, rows, half)
-        gate = logit[cut, :][:, :1] + jnp.sum(took[:, half:], axis=-1, keepdims=True)
-        lanes = split_lanes(gate, (step * rows, extra))
-        d_out[pl.ds(start, step), :, half:] = lanes.reshape(step, rows, extra)
+        took = d_take[pl.ds(start, step)].astype(F32).reshape(step * rows, half)
+        total = (d_keep[cut, :] + took).astype(BF16)
+        d_out[pl.ds(start, step)] = total.reshape(step, rows, half)
 
     chunks(dense_sum)
-    peers(lambda p: send(d_out.at[p], d_in.at[me], d_send.at[p], d_recv.at[me], {"ep": p}).start())
+    peers(lambda p: send(l_out, l_in.at[me], l_send.at[p], l_recv.at[me], {"ep": p}).start(), True)
+    peers(lambda p: send(d_out.at[p], d_in.at[me], d_send.at[p], d_recv.at[me], {"ep": p}).start(), True)
     for key in (("ed", 1), ("ed", 0)):
         loads[key].wait()
 
@@ -208,11 +222,12 @@
         e_out[pl.ds(start, step)] = (own + took).astype(BF16)
 
     chunks(expert_sum)
-    peers(lambda p: send(e_out.at[p], e_in.at[me], e_send.at[p], e_recv.at[me], {"ep": p}).start())
+    peers(lambda p: send(e_out.at[p], e_in.at[me], e_send.at[p], e_recv.at[me], {"ep": p}).start(), True)
 
     small[2].wait()
     small[3].wait()
     d_in[me] = d_out[me]
+    l_in[me] = l_out[...]
     e_in[me] = e_out[me]
 
     diagonal = lax.broadcasted_iota(jnp.int32, (rows, rows), 0) == lax.broadcasted_iota(
@@ -232,27 +247,38 @@
             share = share + jnp.where(named[k] == jnp.asarray(e, F32), factor[k], 0.0)
         return share * e_in[e].astype(F32)
 
+    peers(lambda p: send(l_out, l_in.at[p], l_send.at[p], l_recv.at[p], {"ep": p}).wait_recv())
     peers(lambda p: send(d_out.at[p], d_in.at[p], d_send.at[p], d_recv.at[p], {"ep": p}).wait_recv())
     dense_all = jnp.sum(d_in[...].astype(F32), axis=0)
-    gate_logit = jnp.sum(dense_all[:, half:], axis=-1, keepdims=True)
-    base = jax.nn.sigmoid(gate_logit) * dense_all[:, :half]
+    every = jnp.sum(l_in[...], axis=0)
+    spot = (rows, every.shape[1])
+    mine = lax.broadcasted_iota(jnp.int32, spot, 1) == me * rows + lax.broadcasted_iota(jnp.int32, spot, 0)
+    gate_logit = jnp.sum(jnp.where(mine, every, 0.0), axis=-1, keepdims=True)
+    base = jax.nn.sigmoid(gate_logit) * dense_all
+
+    def gathered(p):
+        to_peer(p, me).wait_send()
+        peer_on(p).wait_send()
+
+    peers(gathered)
 
     def sent(p):
-        send(x_mine.at[me], x_mine.at[me], x_send.at[p], x_recv.at[me], {"ep": p}).wait_send()
-        send(x_mine.at[p], x_mate.at[p], f_send.at[p], f_recv.at[p], {"tp": mate}).wait_send()
+        send(l_out, l_in.at[me], l_send.at[p], l_recv.at[me], {"ep": p}).wait_send()
         send(d_out.at[p], d_in.at[me], d_send.at[p], d_recv.at[me], {"ep": p}).wait_send()
 
     peers(sent)
     d_pair.wait_send()
+    l_pair.wait_send()
     e_pair.wait_send()
 
     def arrived(p):
         send(e_out.at[p], e_in.at[p], e_send.at[p], e_recv.at[p], {"ep": p}).wait_recv()
 
-    if n <= 16:
+    if paired:
         mix = base + scaled(me)
-        for off in offsets:
-            p = lax.rem(me + off, n)
+        order = []
+        peers(order.append)
+        for p in order:
             arrived(p)
             mix = mix + scaled(p)
     else:
@@ -273,12 +299,11 @@
         rows, width = tokens.shape
         half = width // tp
         units, wide = expert_gate.shape[2], dense_gate.shape[1]
-        step = min(n, 8)
+        step = n if n <= 8 else 16
         total = n * rows
         anywhere = pl.BlockSpec(memory_space=pltpu.HBM)
         vmem, dma = pltpu.VMEM, pltpu.SemaphoreType.DMA
         pieces = (n, rows, half)
-        wider = (n, rows, half + extra)
         return pl.pallas_call(
             functools.partial(kernel, n, step),
             out_shape=jax.ShapeDtypeStruct((rows, half), BF16),
@@ -293,12 +318,13 @@
                 vmem((total, units), F32), vmem((total, units), F32),
                 vmem((total, wide), F32), vmem((total, wide), F32),
                 vmem((total, units), BF16), vmem((total, wide), BF16),
-                vmem((total, half), F32), vmem((total, half), F32), vmem((total, extra), F32),
-                vmem(wider, BF16), vmem(wider, BF16), vmem(wider, BF16), vmem(wider, BF16),
+                vmem((total, half), F32), vmem((total, half), F32), vmem((1, total), F32), vmem((1, total), F32), vmem((1, total), F32), vmem((n, 1, total), F32),
+                vmem(pieces, BF16), vmem(pieces, BF16), vmem(pieces, BF16), vmem(pieces, BF16),
                 vmem(pieces, BF16), vmem(pieces, BF16), vmem(pieces, BF16), vmem(pieces, BF16),
                 dma((5,)), dma((12,)),
                 dma((n,)), dma((n,)), dma((n,)), dma((n,)), dma((n,)), dma((n,)), dma((n,)), dma((n,)),
-                dma((2,)), dma((2,)),
+                dma((3,)), dma((3,)),
+                dma((n,)), dma((n,)),
             ],
             compiler_params=pltpu.CompilerParams(
                 collective_id=0, has_side_effects=True, vmem_limit_bytes=vmem_bytes

time: 21.1 us -> 20.6 us (0.976)
  Pallas kernels: 20.3 us -> 19.8 us
    pallas_call x1, Pallas kernels: 20.3 us -> 19.8 us  [per_device(): pl.pallas_call(functools.partial(kernel, n, step), out_shape=jax.ShapeDty...]
where the time goes in v3:
time: 20.6 us; the launch traced here: 20.5 us
  Pallas kernels  19.8 us (96%)
  local copies, waits for them, and re-layouts  0.6 us (3%)
    pallas_call x1, Pallas kernels, per_device(): pl.pallas_call(functools.partial(kernel, n, step), out_shape=jax.ShapeDty...  19.8 us
    unnamed x1, local copies, waits for them, and re-layouts  0.6 us

profile of v3, /device:TPU:0, one launch (start us, length us, event | category | flops | bytes accessed | tf_op | source)
XLA Modules:
  0.0 20.5 jit_solution(13716627523555568675)
XLA Ops:
  0.0 19.8 %shard_map.109 = bf16[8,768]{1,0:T(8,128)(2,1)S(1)} custom-call(bf16[8,1536]{1,0:T(8,128)(2,1)} %tok_hbm.1, f32[1536]{0:T(1024)} %gain_hbm.1, s32[4,8]{1,0:T(4,128)} %bitcast.2, f32[4,8]{1,0:T(4,128)} %bitcast.3, bf16[1,1536,768]{2,1,0:T(8,128)(2,1)} %eg_hbm.1, bf16[1,1536,768]{2,1,0:T(8,128)(2,1)} %eu_hbm.1, bf16[1,768,1536]{2,1,0:T(8,128)(2,1)} %ed_hbm.1, ...), custom_call_target="tpu_custom_call" | custom-call | tf_op jit(solution)/shard_map/pallas_call | solution.py:307
  19.8 0.6 %copy.13 = bf16[8,768]{1,0:T(8,128)(2,1)} copy(bf16[8,768]{1,0:T(8,128)(2,1)S(1)} %shard_map.109) | data formatting | bytes 24576
